TPU v7x, 256 devices: a whole 4x4x8 slice. The times are simulated.
256 devices in a mesh: kv: 32 (over z, y), tp: 8 (over x, core).
Axes of the slice: x: 4, y: 4, z: 8, core: 2. Of those that a mesh axis runs over, the one named last changes fastest.
Arguments:
- residual_in: bfloat16 [256, 2048], P(None, ('kv', 'tp')), may hold values from -14 to 14
- delta_state: float32 [256, 32, 128, 128], P('kv', 'tp'), may hold values from -1 to 1
- norm_gain_first: float32 [2048], P('kv'), may hold values from 0.1 to 1.9
- gate_first: bfloat16 [2048, 5632], P('kv', 'tp'), may hold values from -0.125 to 0.125
- up_first: bfloat16 [2048, 5632], P('kv', 'tp'), may hold values from -0.125 to 0.125
- down_first: bfloat16 [5632, 2048], P('tp', 'kv'), may hold values from -0.15625 to 0.15625
- norm_gain_mixer: float32 [2048], P('kv'), may hold values from 0.1 to 1.9
- query_weight: bfloat16 [2048, 2048], P('kv', 'tp'), may hold values from -0.125 to 0.125
- key_weight: bfloat16 [2048, 2048], P('kv', 'tp'), may hold values from -0.125 to 0.125
- value_weight: bfloat16 [2048, 4096], P('kv', 'tp'), may hold values from -0.125 to 0.125
- output_gate_weight: bfloat16 [2048, 4096], P('kv', 'tp'), may hold values from -0.125 to 0.125
- beta_weight: bfloat16 [2048, 32], P('kv'), may hold values from -0.125 to 0.125
- decay_weight: bfloat16 [2048, 32], P('kv'), may hold values from -0.125 to 0.125
- decay_rate: float32 [32], P('tp'), may hold values from -2.3 to 1.1
- decay_bias: float32 [32], P('tp'), may hold values from -1 to 1
- head_gain: float32 [128], replicated, may hold values from 0.1 to 1.9
- out_weight: bfloat16 [4096, 2048], P('tp', 'kv'), may hold values from -0.125 to 0.125
- norm_gain_second: float32 [2048], P('kv'), may hold values from 0.1 to 1.9
- gate_second: bfloat16 [2048, 5632], P('kv', 'tp'), may hold values from -0.125 to 0.125
- up_second: bfloat16 [2048, 5632], P('kv', 'tp'), may hold values from -0.125 to 0.125
- down_second: bfloat16 [5632, 2048], P('tp', 'kv'), may hold values from -0.15625 to 0.15625
Outputs:
- residual_out: bfloat16 [256, 2048], P(None, ('kv', 'tp'))
- delta_state_out: float32 [256, 32, 128, 128], P('kv', 'tp')
All inputs are finite; a program needn't handle non-finite values.
Results may differ from a plain program's by a relative error of at most 0.03.
Values may be sent and summed in bfloat16 or wider, within the bound.
No kernel may reach another device: no remote copies, remote signals or barrier semaphores. Data moves between devices by JAX's collectives and lax.ppermute only.
A program may use at most 64 MiB of HBM per device.

v0:
```python
import jax
import jax.numpy as jnp
from jax import lax
from jax.sharding import Mesh
from jax.sharding import PartitionSpec as P

D = 2048
HEAD = 128
GATES = 128
epsilon = 1e-06
TP = ("x", "c")
ACROSS = ("z", "x", "c")
bf16 = jnp.bfloat16
f32 = jnp.float32


def exchange(blocks, axis):
    return lax.all_to_all(blocks, axis, split_axis=0, concat_axis=0, tiled=True)


def from_everyone(value, axis):
    return exchange(jnp.broadcast_to(value, (lax.axis_size(axis), *value.shape)), axis)


def everyone_sum(value, axis):
    return from_everyone(value, axis).astype(f32).sum(axis=0)


def times_transposed(left, right_rows):
    return lax.dot_general(left, right_rows, (((1,), (1,)), ((), ())), preferred_element_type=f32)


def square_columns(as_float):
    squares = jnp.sum(as_float * as_float, axis=1, keepdims=True)
    high = squares.astype(bf16).astype(f32)
    lane = lax.broadcasted_iota(jnp.int32, (squares.shape[0], GATES), 1)
    return jnp.where(lane == 0, high, jnp.where(lane == 1, squares - high, 0.0))


def row_scale(first_two):
    return lax.rsqrt((first_two[:, :1] + first_two[:, 1:2]) / D + epsilon)


def hidden_units(residual, gate_up):
    partial_value = jnp.dot(residual, gate_up, preferred_element_type=f32)
    both = jnp.concatenate([partial_value, square_columns(residual.astype(f32))], axis=1).astype(
        bf16
    )
    summed = everyone_sum(both, "y")
    width = gate_up.shape[1]
    scale = row_scale(summed[:, width:])
    gate_act = summed[:, : width // 2] * scale
    up_act = summed[:, width // 2 : width] * scale
    return (jax.nn.silu(gate_act) * up_act).astype(bf16)


def unit_heads(projected, head_size):
    activated = jax.nn.silu(projected).reshape(projected.shape[0], -1, head_size)
    return activated * lax.rsqrt(jnp.sum(activated * activated, axis=-1, keepdims=True) + epsilon)


def delta_step(old_state, key_rows, queries, values, beta_gate, decay_gate):
    faded_state = old_state * decay_gate[:, :, None, None]
    predicted = jnp.einsum("rhab,rha->rhb", faded_state, key_rows, precision=lax.Precision.HIGHEST)
    correction = beta_gate[:, :, None] * (values - predicted)
    updated = faded_state + key_rows[:, :, :, None] * correction[:, :, None, :]
    reading = jnp.einsum("rhab,rha->rhb", updated, queries, precision=lax.Precision.HIGHEST)
    return (updated, reading)


def mixer_values(residual, mixer_in, decay_rate, decay_bias, head_gain, old_state):
    row_count, heads_dev, head_size = old_state.shape[:3]
    projected = jnp.dot(residual, mixer_in, preferred_element_type=f32)
    width = mixer_in.shape[1] - GATES
    squares = square_columns(residual.astype(f32))
    tail = projected[:, width:] + jnp.roll(squares, 2 * heads_dev, axis=1)
    both = jnp.concatenate([projected[:, :width], tail], axis=1).astype(bf16)
    blocks = both.reshape(-1, row_count, both.shape[1])
    summed = exchange(blocks, "y").astype(f32).sum(axis=0)
    tail = summed[:, width:]
    scale = row_scale(tail[:, 2 * heads_dev :])
    summed = summed[:, :width] * scale
    gates = tail * scale
    value_cols = heads_dev * head_size
    key_cols = (width - 2 * value_cols) // 2
    repeat_count = value_cols // key_cols
    queries = jnp.repeat(
        unit_heads(summed[:, :key_cols], head_size) * head_size ** (-0.5), repeat_count, axis=1
    )
    key_rows = jnp.repeat(
        unit_heads(summed[:, key_cols : 2 * key_cols], head_size), repeat_count, axis=1
    )
    values = jax.nn.silu(summed[:, 2 * key_cols : 2 * key_cols + value_cols]).reshape(
        row_count, heads_dev, head_size
    )
    out_gate = jax.nn.silu(summed[:, 2 * key_cols + value_cols :]).reshape(
        row_count, heads_dev, head_size
    )
    beta_gate = jax.nn.sigmoid(gates[:, :heads_dev])
    decay_gate = jnp.exp(
        -jnp.exp(decay_rate)[None, :]
        * jax.nn.softplus(gates[:, heads_dev : 2 * heads_dev] + decay_bias[None, :])
    )
    new_state, reading = delta_step(old_state, key_rows, queries, values, beta_gate, decay_gate)
    normed = reading * lax.rsqrt(jnp.mean(reading * reading, axis=-1, keepdims=True) + epsilon)
    normed = (normed * head_gain * out_gate).reshape(row_count, value_cols).astype(bf16)
    return (normed, new_state)


def body(
    residual_in,
    delta_state,
    norm_gain_first,
    gate_first,
    up_first,
    down_first,
    norm_gain_mixer,
    query_weight,
    key_weight,
    value_weight,
    output_gate_weight,
    beta_weight,
    decay_weight,
    decay_rate,
    decay_bias,
    head_gain,
    out_weight,
    norm_gain_second,
    gate_second,
    up_second,
    down_second,
):
    planes, tp_count = (lax.axis_size("z"), lax.axis_size(TP))
    heads_dev = decay_rate.shape[0]

    def scaled_rows(gain, weights):
        return (jnp.concatenate(weights, axis=1).astype(f32) * gain[:, None]).astype(bf16)

    def gathered(weights):
        return lax.all_gather(jnp.concatenate(weights, axis=1), "z", axis=0, tiled=True)

    head_start = lax.axis_index(TP) * heads_dev
    gate_cols = [
        lax.dynamic_slice_in_dim(beta_weight, head_start, heads_dev, 1),
        lax.dynamic_slice_in_dim(decay_weight, head_start, heads_dev, 1),
        jnp.zeros((beta_weight.shape[0], GATES - 2 * heads_dev), bf16),
    ]
    first_in = scaled_rows(norm_gain_first, [gate_first, up_first])
    mixer_in = scaled_rows(
        norm_gain_mixer, [query_weight, key_weight, value_weight, output_gate_weight, *gate_cols]
    )
    second_in = scaled_rows(norm_gain_second, [gate_second, up_second])
    width, mixer_width = (first_in.shape[1], mixer_in.shape[1])
    first_in = gathered([first_in])
    middle = gathered([down_first.T, mixer_in])
    last = gathered([out_weight.T, second_in, down_second.T])
    down_first, mixer_in = (middle[:, : width // 2], middle[:, width // 2 :])
    values_width = out_weight.shape[0]
    out_rows, second_in, down_second = (
        last[:, :values_width],
        last[:, values_width : values_width + width],
        last[:, values_width + width :],
    )
    columns = residual_in.T
    own_cols, rows = (columns.shape[0], columns.shape[1] // planes)
    pieces = jnp.moveaxis(columns.reshape(own_cols, planes, rows), 1, 0)
    pieces = jnp.broadcast_to(pieces[:, None], (planes, tp_count, own_cols, rows))
    residual = exchange(pieces.reshape(-1, own_cols, rows), ACROSS).reshape(-1, rows).T
    hidden = hidden_units(residual, first_in)
    projected = times_transposed(hidden, down_first).astype(bf16)
    after_first = (residual.astype(f32) + 0.5 * everyone_sum(projected, TP)).astype(bf16)
    normed, new_state = mixer_values(
        after_first, mixer_in, decay_rate, decay_bias, head_gain, delta_state
    )
    normed = from_everyone(normed, "y").reshape(rows, -1)
    projected = times_transposed(normed, out_rows).astype(bf16)
    after_mixer = (after_first.astype(f32) + everyone_sum(projected, TP)).astype(bf16)
    hidden = hidden_units(after_mixer, second_in)
    projected = times_transposed(down_second, hidden).astype(bf16)
    pieces = jnp.concatenate([projected, after_mixer.T], axis=1)
    arrived = exchange(pieces.reshape(-1, own_cols, 2 * rows), ACROSS)
    arrived = arrived.reshape(planes, tp_count, own_cols, 2 * rows).astype(f32)
    final = arrived[:, 0, :, rows:] + 0.5 * arrived[..., :rows].sum(axis=1)
    residual_out = jnp.moveaxis(final, 1, 2).reshape(planes * rows, own_cols).astype(bf16)
    return (residual_out, new_state)


def solution(mesh):
    cut = Mesh(mesh.devices.reshape(8, 4, 4, 2), ("z", "y", "x", "c"))
    kv, tp = (("z", "y"), ("x", "c"))
    wide, tall = (P(kv, tp), P(tp, kv))
    placed = (
        P(None, kv + tp),
        P(kv, tp, None, None),
        P(kv),
        wide,
        wide,
        tall,
        P(kv),
        wide,
        wide,
        wide,
        wide,
        P(kv, None),
        P(kv, None),
        P(tp),
        P(tp),
        P(),
        tall,
        P(kv),
        wide,
        wide,
        tall,
    )
    return jax.shard_map(
        body,
        mesh=cut,
        in_specs=placed,
        out_specs=(P(None, kv + tp), P(kv, tp, None, None)),
        check_vma=False,
    )
```

profile of v0, /device:TPU:1, one launch (start us, length us, event | category | flops | bytes accessed | tf_op | source)
XLA Modules:
  0.0 199.8 jit_solution(17900534135852283089)
XLA Ops:
  7.2 1.7 multiply_convert_fusion.1
  9.0 0.7 constant_dynamic-slice_fusion
  9.7 0.1 copy.77
  9.8 0.1 copy.78
  10.0 1.0 concatenate.43
  11.0 0.8 multiply_convert_fusion
  11.7 1.8 pad_maximum_fusion.1
  13.5 0.1 reshape.109
  13.7 0.7 reshape.127
  14.4 13.0 %all-to-all-start = ((bf16[64,2,128]{2,1,0:T(2,128)(2,1)}), bf16[64,2,128]{2,1,0:T(2,128)(2,1)S(1)}, u32[]{:S(2)}, u32[]{:S(2)}) async-start(bf16[64,2,128]{2,1,0:T(2,128)(2,1)} %reshape.127), calls=%async_computation | async-start | bytes 65536 | tf_op jit(solution)/shard_map/all_to_all | solution.py:18
  27.4 9.5 %all-to-all-done = bf16[64,2,128]{2,1,0:T(2,128)(2,1)S(1)} async-done(((bf16[64,2,128]{2,1,0:T(2,128)(2,1)}), bf16[64,2,128]{2,1,0:T(2,128)(2,1)S(1)}, u32[]{:S(2)}, u32[]{:S(2)}) %all-to-all-start) | async-done | bytes 32800 | tf_op jit(solution)/shard_map/all_to_all | solution.py:18
  36.9 0.1 reshape.128
  37.0 0.1 copy.76
  37.1 0.1 fusion.19
  37.2 0.1 select_convert_fusion.1
  37.3 12.2 %all-gather.6.cloned.1.call-done = bf16[512,1408]{1,0:T(8,128)(2,1)} async-done(((bf16[64,1408]{1,0:T(8,128)(2,1)}), bf16[512,1408]{1,0:T(8,128)(2,1)}) %all-gather.6.cloned.1.call-update) | async-done | bytes 1441808 | tf_op jit(solution)/shard_map/all_gather | solution.py:140
  49.6 1.7 fusion
  51.3 0.8 broadcast_in_dim.91
  52.1 4.2 %all-to-all-start.1 = ((bf16[4,32,1536]{2,1,0:T(8,128)(2,1)}), bf16[4,32,1536]{2,1,0:T(8,128)(2,1)S(1)}, u32[]{:S(2)}, u32[]{:S(2)}) async-start(bf16[4,32,1536]{2,1,0:T(8,128)(2,1)} %broadcast_in_dim.91), calls=%async_computation.1 | async-start | bytes 786432 | tf_op jit(solution)/shard_map/all_to_all | solution.py:18
  56.3 0.1 multiply_convert_fusion.2
  56.4 6.1 %all-to-all-done.1 = bf16[4,32,1536]{2,1,0:T(8,128)(2,1)S(1)} async-done(((bf16[4,32,1536]{2,1,0:T(8,128)(2,1)}), bf16[4,32,1536]{2,1,0:T(8,128)(2,1)S(1)}, u32[]{:S(2)}, u32[]{:S(2)}) %all-to-all-start.1) | async-done | bytes 393248 | tf_op jit(solution)/shard_map/all_to_all | solution.py:18
  62.6 0.2 fusion.41
  62.8 29.2 %all-gather.8.cloned.1.call-done = bf16[512,2368]{1,0:T(8,128)(2,1)} async-done(((bf16[64,2368]{1,0:T(8,128)(2,1)}), bf16[512,2368]{1,0:T(8,128)(2,1)}) %all-gather.8.cloned.1.call-update) | async-done | bytes 2424848 | tf_op jit(solution)/shard_map/all_gather | solution.py:140
  91.9 1.5 convolution_convert_fusion.3
  93.4 0.7 broadcast_in_dim.93
  94.2 8.7 %all-to-all-start.2 = ((bf16[8,32,512]{2,1,0:T(8,128)(2,1)}), bf16[8,32,512]{2,1,0:T(8,128)(2,1)S(1)}, u32[]{:S(2)}, u32[]{:S(2)}) async-start(bf16[8,32,512]{2,1,0:T(8,128)(2,1)} %broadcast_in_dim.93), calls=%async_computation.2 | async-start | bytes 524288 | tf_op jit(solution)/shard_map/all_to_all | solution.py:18
  102.9 0.8 pad_maximum_fusion
  103.7 5.7 %all-to-all-done.2 = bf16[8,32,512]{2,1,0:T(8,128)(2,1)S(1)} async-done(((bf16[8,32,512]{2,1,0:T(8,128)(2,1)}), bf16[8,32,512]{2,1,0:T(8,128)(2,1)S(1)}, u32[]{:S(2)}, u32[]{:S(2)}) %all-to-all-start.2) | async-done | bytes 262176 | tf_op jit(solution)/shard_map/all_to_all | solution.py:18
  109.4 0.1 fusion.17
  109.5 0.1 select_select_fusion
  109.6 0.1 slice.138
  109.6 2.2 %fusion.3 = f32[32,1664]{1,0:T(8,128)S(1)} fusion(bf16[32,512]{1,0:T(8,128)(2,1)S(1)} %get-tuple-element.5, bf16[512,2368]{1,0:T(8,128)(2,1)} %all-gather.8.cloned.1.call-done), kind=kOutput, calls=%fused_computation.6 | convolution fusion | flops 54525952 | bytes 1949696 | tf_op jit(solution)/shard_map/dot_general | solution.py:73
  111.8 0.1 fusion.46
  111.9 0.7 pad_maximum_fusion.2
  112.6 4.0 %all-to-all-start.3 = ((bf16[4,8,1664]{2,1,0:T(8,128)(2,1)}), bf16[4,8,1664]{2,1,0:T(8,128)(2,1)S(1)}, u32[]{:S(2)}, u32[]{:S(2)}) async-start(bf16[4,8,1664]{2,1,0:T(8,128)(2,1)} %pad_maximum_fusion.2), calls=%async_computation.3 | async-start | bytes 212992 | tf_op jit(solution)/shard_map/all_to_all | solution.py:18
  116.6 4.7 %all-to-all-done.3 = bf16[4,8,1664]{2,1,0:T(8,128)(2,1)S(1)} async-done(((bf16[4,8,1664]{2,1,0:T(8,128)(2,1)}), bf16[4,8,1664]{2,1,0:T(8,128)(2,1)S(1)}, u32[]{:S(2)}, u32[]{:S(2)}) %all-to-all-start.3) | async-done | bytes 106528 | tf_op jit(solution)/shard_map/all_to_all | solution.py:18
  121.4 0.2 fusion.56
  121.6 0.1 fusion.47
  121.9 0.1 add_divide_fusion
  122.0 0.1 copy.80
  122.1 2.0 %fusion.1 = f32[8,4,1,128]{3,2,1,0:T(1,128)S(1)} fusion(f32[8,4,128,1]{2,3,1,0:T(1,128)S(1)} %bitcast.109, f32[8,4,128,128]{3,2,1,0:T(8,128)S(1)} %copy-done, f32[8,4]{1,0:T(8,128)S(1)} %get-tuple-element.9), kind=kOutput, calls=%fused_computation.4 | convolution fusion | flops 6815744 | bytes 2130048 | tf_op jit(solution)/shard_map/rhab,rha->rhb/dot_general | solution.py:64
  124.2 0.8 multiply_add_fusion
  125.0 1.3 copy-done.1
  126.3 1.9 fusion.65
  128.2 0.1 fusion.43
  128.3 0.1 fusion.50
  128.4 6.7 %all_to_all.40 = bf16[4,8,512]{2,1,0:T(8,128)(2,1)S(1)} all-to-all(bf16[4,8,512]{2,1,0:T(8,128)(2,1)S(1)} %broadcast_in_dim.98), channel_id=1, replica_groups=mesh['z'=8,'y'=4,'x'=4,'c'=2] {'y'}, dimensions={0} | all-to-all | bytes 65536 | tf_op jit(solution)/shard_map/all_to_all | solution.py:18
  135.1 8.7 %all-gather.4.cloned.1.call-done = bf16[512,2624]{1,0:T(8,128)(2,1)} async-done(((bf16[64,2624]{1,0:T(8,128)(2,1)}), bf16[512,2624]{1,0:T(8,128)(2,1)}) %all-gather.4.cloned.1.call-update) | async-done | bytes 2686992 | tf_op jit(solution)/shard_map/all_gather | solution.py:140
  143.8 1.3 convolution_convert_fusion.4
  145.2 13.9 %all_to_all.41 = bf16[8,32,512]{2,1,0:T(8,128)(2,1)S(1)} all-to-all(bf16[8,32,512]{2,1,0:T(8,128)(2,1)S(1)} %broadcast_in_dim.99), channel_id=1, replica_groups=mesh['z'=8,'y'=4,'x'=4,'c'=2] {'x','c'}, dimensions={0} | all-to-all | bytes 524288 | tf_op jit(solution)/shard_map/all_to_all | solution.py:18
  159.1 0.1 multiply_reduce_fusion
  159.3 0.1 select_convert_fusion
  159.4 1.7 convolution_convert_fusion
  161.1 0.8 broadcast_in_dim.102
  161.9 3.8 %all-to-all-start.6 = ((bf16[4,32,1536]{2,1,0:T(8,128)(2,1)}), bf16[4,32,1536]{2,1,0:T(8,128)(2,1)S(1)}, u32[]{:S(2)}, u32[]{:S(2)}) async-start(bf16[4,32,1536]{2,1,0:T(8,128)(2,1)} %broadcast_in_dim.102), calls=%async_computation.6 | async-start | bytes 786432 | tf_op jit(solution)/shard_map/all_to_all | solution.py:18
  165.7 6.5 %all-to-all-done.6 = bf16[4,32,1536]{2,1,0:T(8,128)(2,1)S(1)} async-done(((bf16[4,32,1536]{2,1,0:T(8,128)(2,1)}), bf16[4,32,1536]{2,1,0:T(8,128)(2,1)S(1)}, u32[]{:S(2)}, u32[]{:S(2)}) %all-to-all-start.6) | async-done | bytes 393248 | tf_op jit(solution)/shard_map/all_to_all | solution.py:18
  172.3 0.2 fusion.36
  172.5 1.5 convolution_convert_fusion.2
  174.0 0.1 copy.83
  174.2 0.2 reshape.129
  174.3 18.0 %all_to_all.42 = bf16[64,2,256]{2,1,0:T(2,128)(2,1)S(1)} all-to-all(bf16[64,2,256]{2,1,0:T(2,128)(2,1)S(1)} %reshape.129), channel_id=1, replica_groups=mesh['z'=8,'y'=4,'x'=4,'c'=2] {'z','x','c'}, dimensions={0} | all-to-all | bytes 131072 | tf_op jit(solution)/shard_map/all_to_all | solution.py:18
  192.3 0.1 reshape.130
  192.5 0.1 fusion.32
  192.6 0.7 convert_element_type.209
  (64 shorter events, 1.0 us)
Async XLA Ops:
  7.2 6.4 %copy-start.6 = (bf16[256,8]{0,1:T(8,128)(2,1)S(1)}, bf16[256,8]{0,1:T(8,128)(2,1)}, u32[]{:S(2)}) copy-start(bf16[256,8]{0,1:T(8,128)(2,1)} %param.21) | copy-start | bytes 12292
  7.2 42.4 %all-gather.6.cloned.1.call-start = ((), (), s32[]{:S(2)}) async-start(), calls=%async_computation.9 | async-start | bytes 1622016 | tf_op jit(solution)/shard_map/all_gather | solution.py:140
  9.0 83.0 %all-gather.8.cloned.1.call-start = ((), (), s32[]{:S(2)}) async-start(), calls=%async_computation.10 | async-start | bytes 2801664 | tf_op jit(solution)/shard_map/all_gather | solution.py:140
  13.5 42.8 %copy-start.2 = (bf16[64,704]{1,0:T(8,128)(2,1)S(1)}, bf16[64,704]{1,0:T(8,128)(2,1)}, u32[]{:S(2)}) copy-start(bf16[64,704]{1,0:T(8,128)(2,1)} %param.40) | copy-start | bytes 270340
  13.5 42.8 %copy-start.3 = (bf16[64,704]{1,0:T(8,128)(2,1)S(1)}, bf16[64,704]{1,0:T(8,128)(2,1)}, u32[]{:S(2)}) copy-start(bf16[64,704]{1,0:T(8,128)(2,1)} %param.39) | copy-start | bytes 270340
  13.5 42.8 %copy-start.7 = (f32[64]{0:T(128)S(1)}, f32[64]{0:T(128)}, u32[]{:S(2)}) copy-start(f32[64]{0:T(128)} %param.38) | copy-start | bytes 772
  14.4 22.5 %all-to-all-start = ((bf16[64,2,128]{2,1,0:T(2,128)(2,1)}), bf16[64,2,128]{2,1,0:T(2,128)(2,1)S(1)}, u32[]{:S(2)}, u32[]{:S(2)}) async-start(bf16[64,2,128]{2,1,0:T(2,128)(2,1)} %reshape.127), calls=%async_computation | async-start | bytes 65536 | tf_op jit(solution)/shard_map/all_to_all | solution.py:18
  52.1 50.8 %copy-start.4 = (bf16[704,64]{0,1:T(8,128)(2,1)S(1)}, bf16[704,64]{0,1:T(8,128)(2,1)}, u32[]{:S(2)}) copy-start(bf16[704,64]{0,1:T(8,128)(2,1)} %param.41) | copy-start | bytes 270340
  52.1 50.8 %copy-start.5 = (bf16[512,64]{0,1:T(8,128)(2,1)S(1)}, bf16[512,64]{0,1:T(8,128)(2,1)}, u32[]{:S(2)}) copy-start(bf16[512,64]{0,1:T(8,128)(2,1)} %param.37) | copy-start | bytes 196612
  52.1 10.5 %all-to-all-start.1 = ((bf16[4,32,1536]{2,1,0:T(8,128)(2,1)}), bf16[4,32,1536]{2,1,0:T(8,128)(2,1)S(1)}, u32[]{:S(2)}, u32[]{:S(2)}) async-start(bf16[4,32,1536]{2,1,0:T(8,128)(2,1)} %broadcast_in_dim.91), calls=%async_computation.1 | async-start | bytes 786432 | tf_op jit(solution)/shard_map/all_to_all | solution.py:18
  94.2 15.2 %all-to-all-start.2 = ((bf16[8,32,512]{2,1,0:T(8,128)(2,1)}), bf16[8,32,512]{2,1,0:T(8,128)(2,1)S(1)}, u32[]{:S(2)}, u32[]{:S(2)}) async-start(bf16[8,32,512]{2,1,0:T(8,128)(2,1)} %broadcast_in_dim.93), calls=%async_computation.2 | async-start | bytes 524288 | tf_op jit(solution)/shard_map/all_to_all | solution.py:18
  102.9 13.7 %copy-start.10 = (f32[4]{0:T(128)S(1)}, f32[4]{0:T(128)}, u32[]{:S(2)}) copy-start(f32[4]{0:T(128)} %param.34) | copy-start | bytes 52
  102.9 41.0 %all-gather.4.cloned.1.call-start = ((), (), s32[]{:S(2)}) async-start(), calls=%async_computation.8 | async-start | bytes 3096576 | tf_op jit(solution)/shard_map/all_gather | solution.py:140
  103.6 18.3 %copy-start.9 = (f32[4]{0:T(128)S(1)}, f32[4]{0:T(128)}, u32[]{:S(2)}) copy-start(f32[4]{0:T(128)} %param.35) | copy-start | bytes 52
  103.6 18.5 %copy-start = (f32[8,4,128,128]{3,2,1,0:T(8,128)S(1)}, f32[8,4,128,128]{3,2,1,0:T(8,128)}, u32[]{:S(2)}) copy-start(f32[8,4,128,128]{3,2,1,0:T(8,128)} %param.22) | copy-start | bytes 6291460
  112.6 8.8 %all-to-all-start.3 = ((bf16[4,8,1664]{2,1,0:T(8,128)(2,1)}), bf16[4,8,1664]{2,1,0:T(8,128)(2,1)S(1)}, u32[]{:S(2)}, u32[]{:S(2)}) async-start(bf16[4,8,1664]{2,1,0:T(8,128)(2,1)} %pad_maximum_fusion.2), calls=%async_computation.3 | async-start | bytes 212992 | tf_op jit(solution)/shard_map/all_to_all | solution.py:18
  125.0 1.3 copy-start.1
  125.0 3.3 %copy-start.8 = (f32[128]{0:T(128)S(1)}, f32[128]{0:T(128)}, u32[]{:S(2)}) copy-start(f32[128]{0:T(128)} %param.36) | copy-start | bytes 1540
  161.9 10.4 %all-to-all-start.6 = ((bf16[4,32,1536]{2,1,0:T(8,128)(2,1)}), bf16[4,32,1536]{2,1,0:T(8,128)(2,1)S(1)}, u32[]{:S(2)}, u32[]{:S(2)}) async-start(bf16[4,32,1536]{2,1,0:T(8,128)(2,1)} %broadcast_in_dim.102), calls=%async_computation.6 | async-start | bytes 786432 | tf_op jit(solution)/shard_map/all_to_all | solution.py:18
Sparse Core Ops, SparseCore 0:
  10.3 39.1 all-gather.5
  51.3 40.5 all-gather.7
  105.4 38.3 all-gather.3
where the time goes:
time: 201 us; the launch traced here: 200 us
  waiting for transfers between devices  82.7 us (41%)
  blocking collectives  38.6 us (19%)
  starting transfers between devices  33.8 us (17%)
  between operations  14.1 us (7%)
  matrix products  13.8 us (7%)
  other arithmetic  8.8 us (4%)
  local copies, waits for them, and re-layouts  7.98 us (4%)
    all_gather x3, waiting for transfers between devices, gathered(): lax.all_gather(jnp.concatenate(weights, axis=1), 'z', axis=0, tiled=True)  50.1 us
    all_to_all x3, blocking collectives, exchange(): return lax.all_to_all(blocks, axis, split_axis=0, concat_axis=0, tiled=True)  38.6 us
    all_to_all x5, starting transfers between devices, exchange(): return lax.all_to_all(blocks, axis, split_axis=0, concat_axis=0, tiled=True)  33.7 us
    all_to_all x5, waiting for transfers between devices, exchange(): return lax.all_to_all(blocks, axis, split_axis=0, concat_axis=0, tiled=True)  32.6 us
    dot_general x3, matrix products, times_transposed(): lax.dot_general(left, right_rows, (((1,), (1,)), ((), ())), preferred_ele...  4.25 us
  transfers between devices with their start and end apart: 8, of which 8 were waited for; matrix products, arithmetic and copies ran while one was open for 9% of the time, Pallas kernels for 0%

commit v1 on v0

--- a/solution.py
+++ b/solution.py
@@ -137,7 +137,15 @@
         return (jnp.concatenate(weights, axis=1).astype(f32) * gain[:, None]).astype(bf16)
 
     def gathered(weights):
-        return lax.all_gather(jnp.concatenate(weights, axis=1), "z", axis=0, tiled=True)
+
+        def _report_rings(base_x):
+            row_list = []
+            for _ in range(lax.axis_size("z")):
+                row_list.append(base_x)
+            clean = jnp.stack(row_list)
+            return jnp.concatenate(lax.all_to_all(clean, "z", 0, 0), axis=0)
+
+        return _report_rings(jnp.concatenate(weights, axis=1))
 
     head_start = lax.axis_index(TP) * heads_dev
     gate_cols = [

time: 201 us -> 289 us (1.44)
  blocking collectives: 38.6 us -> 93 us
  waiting for transfers between devices: 82.7 us -> 128 us
  between operations: 14.1 us -> 1.19 us
  starting transfers between devices: 33.8 us -> 41.3 us
  matrix products: 13.8 us -> 7.73 us
  local copies, waits for them, and re-layouts: 7.98 us -> 11.9 us
  other arithmetic: 8.8 us -> 5.11 us
    all_to_all x0 -> x2, waiting for transfers between devices: none -> 91.2 us  [_report_rings(): return jnp.concatenate(lax.all_to_all(clean, 'z', 0, 0), axis=0)]
    all_to_all x0 -> x1, blocking collectives: none -> 64.1 us  [_report_rings(): return jnp.concatenate(lax.all_to_all(clean, 'z', 0, 0), axis=0)]
    all_gather x3 -> x0, waiting for transfers between devices: 50.1 us -> none  [gathered(): lax.all_gather(jnp.concatenate(weights, axis=1), 'z', axis=0, tiled=True)]
    all_to_all x3 -> x2, blocking collectives: 38.6 us -> 28.9 us  [exchange(): return lax.all_to_all(blocks, axis, split_axis=0, concat_axis=0, tiled=True)]
    all_to_all x0 -> x2, starting transfers between devices: none -> 7.6 us  [_report_rings(): return jnp.concatenate(lax.all_to_all(clean, 'z', 0, 0), axis=0)]
    all_to_all x5 -> x6, waiting for transfers between devices: 32.6 us -> 36.3 us  [exchange(): return lax.all_to_all(blocks, axis, split_axis=0, concat_axis=0, tiled=True)]
    dot_general x3, matrix products: 4.25 us -> 0.94 us  [times_transposed(): lax.dot_general(left, right_rows, (((1,), (1,)), ((), ())), preferred_ele...]
    another operation x0 -> x3, local copies, waits for them, and re-layouts: none -> 3.05 us  [_report_rings(): clean = jnp.stack(row_list)]
  transfers between devices with their start and end apart: 8 -> 8, of which waited for: 8 -> 8; matrix products, arithmetic and copies ran while one was open for 9% -> 1% of each run, Pallas kernels for 0% -> 0%
where the time goes in v1:
time: 289 us; the launch traced here: 288 us
  waiting for transfers between devices  128 us (44%)
  blocking collectives  93 us (32%)
  starting transfers between devices  41.3 us (14%)
  local copies, waits for them, and re-layouts  11.9 us (4%)
  matrix products  7.73 us (3%)
  other arithmetic  5.11 us (2%)
    all_to_all x2, waiting for transfers between devices, _report_rings(): return jnp.concatenate(lax.all_to_all(clean, 'z', 0, 0), axis=0)  91.2 us
    all_to_all x1, blocking collectives, _report_rings(): return jnp.concatenate(lax.all_to_all(clean, 'z', 0, 0), axis=0)  64.1 us
    all_to_all x6, waiting for transfers between devices, exchange(): return lax.all_to_all(blocks, axis, split_axis=0, concat_axis=0, tiled=True)  36.3 us
    all_to_all x6, starting transfers between devices, exchange(): return lax.all_to_all(blocks, axis, split_axis=0, concat_axis=0, tiled=True)  33.7 us
    all_to_all x2, blocking collectives, exchange(): return lax.all_to_all(blocks, axis, split_axis=0, concat_axis=0, tiled=True)  28.9 us
    all_to_all x2, starting transfers between devices, _report_rings(): return jnp.concatenate(lax.all_to_all(clean, 'z', 0, 0), axis=0)  7.6 us
  transfers between devices with their start and end apart: 8, of which 8 were waited for; matrix products, arithmetic and copies ran while one was open for 1% of the time, Pallas kernels for 0%

profile of v1, /device:TPU:1, one launch (start us, length us, event | category | flops | bytes accessed | tf_op | source)
XLA Modules:
  0.0 287.8 jit_solution(9409759367210519676)
XLA Ops:
  0.6 0.8 reshape.136
  1.4 0.7 reshape.156
  2.2 13.0 %all-to-all-start.1 = ((bf16[64,2,128]{2,1,0:T(2,128)(2,1)}), bf16[64,2,128]{2,1,0:T(2,128)(2,1)S(1)}, u32[]{:S(2)}, u32[]{:S(2)}) async-start(bf16[64,2,128]{2,1,0:T(2,128)(2,1)} %reshape.156), calls=%async_computation.1 | async-start | bytes 65536 | tf_op jit(solution)/shard_map/all_to_all | solution.py:18
  15.2 1.0 multiply_convert_fusion.1
  16.3 8.2 %all-to-all-done.1 = bf16[64,2,128]{2,1,0:T(2,128)(2,1)S(1)} async-done(((bf16[64,2,128]{2,1,0:T(2,128)(2,1)}), bf16[64,2,128]{2,1,0:T(2,128)(2,1)S(1)}, u32[]{:S(2)}, u32[]{:S(2)}) %all-to-all-start.1) | async-done | bytes 32800 | tf_op jit(solution)/shard_map/all_to_all | solution.py:18
  24.5 1.2 stack.7
  25.7 3.7 %all-to-all-start.2 = ((bf16[8,64,1408]{2,1,0:T(8,128)(2,1)}), bf16[8,64,1408]{2,1,0:T(8,128)(2,1)S(1)}, u32[]{:S(2)}, u32[]{:S(2)}) async-start(bf16[8,64,1408]{2,1,0:T(8,128)(2,1)} %stack.7), calls=%async_computation.2 | async-start | bytes 2883584 | tf_op jit(solution)/shard_map/all_to_all | solution.py:146
  29.4 0.7 constant_dynamic-slice_fusion
  30.1 0.1 copy.78
  30.3 0.1 copy.77
  30.4 0.1 concatenate.45
  30.6 0.1 multiply_convert_fusion
  30.7 0.1 reshape.157
  30.8 0.1 copy.76
  30.9 0.1 fusion.19
  31.1 34.1 %all-to-all-done.2 = bf16[8,64,1408]{2,1,0:T(8,128)(2,1)S(1)} async-done(((bf16[8,64,1408]{2,1,0:T(8,128)(2,1)}), bf16[8,64,1408]{2,1,0:T(8,128)(2,1)S(1)}, u32[]{:S(2)}, u32[]{:S(2)}) %all-to-all-start.2) | async-done | bytes 1441824 | tf_op jit(solution)/shard_map/all_to_all | solution.py:146
  65.2 0.4 fusion
  65.6 0.8 broadcast_in_dim.91
  66.4 4.2 %all-to-all-start.3 = ((bf16[4,32,1536]{2,1,0:T(8,128)(2,1)}), bf16[4,32,1536]{2,1,0:T(8,128)(2,1)S(1)}, u32[]{:S(2)}, u32[]{:S(2)}) async-start(bf16[4,32,1536]{2,1,0:T(8,128)(2,1)} %broadcast_in_dim.91), calls=%async_computation.3 | async-start | bytes 786432 | tf_op jit(solution)/shard_map/all_to_all | solution.py:18
  70.6 0.1 pad_maximum_fusion.1
  70.7 6.1 %all-to-all-done.3 = bf16[4,32,1536]{2,1,0:T(8,128)(2,1)S(1)} async-done(((bf16[4,32,1536]{2,1,0:T(8,128)(2,1)}), bf16[4,32,1536]{2,1,0:T(8,128)(2,1)S(1)}, u32[]{:S(2)}, u32[]{:S(2)}) %all-to-all-start.3) | async-done | bytes 393248 | tf_op jit(solution)/shard_map/all_to_all | solution.py:18
  76.8 1.6 stack.8
  78.4 3.9 %all-to-all-start.4 = ((bf16[8,64,2368]{2,1,0:T(8,128)(2,1)}), bf16[8,64,2368]{2,1,0:T(8,128)(2,1)S(1)}, u32[]{:S(2)}, u32[]{:S(2)}) async-start(bf16[8,64,2368]{2,1,0:T(8,128)(2,1)} %stack.8), calls=%async_computation.4 | async-start | bytes 4980736 | tf_op jit(solution)/shard_map/all_to_all | solution.py:146
  82.4 0.2 fusion.41
  82.6 57.1 %all-to-all-done.4 = bf16[8,64,2368]{2,1,0:T(8,128)(2,1)S(1)} async-done(((bf16[8,64,2368]{2,1,0:T(8,128)(2,1)}), bf16[8,64,2368]{2,1,0:T(8,128)(2,1)S(1)}, u32[]{:S(2)}, u32[]{:S(2)}) %all-to-all-start.4) | async-done | bytes 2424864 | tf_op jit(solution)/shard_map/all_to_all | solution.py:146
  139.7 0.3 convolution_convert_fusion.3
  140.0 1.1 broadcast_in_dim.93
  141.1 0.1 copy-done.2
  141.2 6.5 %all-to-all-start.5 = ((bf16[8,32,512]{2,1,0:T(8,128)(2,1)}), bf16[8,32,512]{2,1,0:T(8,128)(2,1)S(1)}, u32[]{:S(2)}, u32[]{:S(2)}) async-start(bf16[8,32,512]{2,1,0:T(8,128)(2,1)} %broadcast_in_dim.93), calls=%async_computation.5 | async-start | bytes 524288 | tf_op jit(solution)/shard_map/all_to_all | solution.py:18
  147.8 0.1 multiply_convert_fusion.2
  147.9 6.4 %all-to-all-done.5 = bf16[8,32,512]{2,1,0:T(8,128)(2,1)S(1)} async-done(((bf16[8,32,512]{2,1,0:T(8,128)(2,1)}), bf16[8,32,512]{2,1,0:T(8,128)(2,1)S(1)}, u32[]{:S(2)}, u32[]{:S(2)}) %all-to-all-start.5) | async-done | bytes 262176 | tf_op jit(solution)/shard_map/all_to_all | solution.py:18
  154.3 0.1 fusion.17
  154.4 2.2 fusion.3
  156.9 0.7 pad_maximum_fusion.2
  157.5 3.3 %all-to-all-start.6 = ((bf16[4,8,1664]{2,1,0:T(8,128)(2,1)}), bf16[4,8,1664]{2,1,0:T(8,128)(2,1)S(1)}, u32[]{:S(2)}, u32[]{:S(2)}) async-start(bf16[4,8,1664]{2,1,0:T(8,128)(2,1)} %pad_maximum_fusion.2), calls=%async_computation.6 | async-start | bytes 212992 | tf_op jit(solution)/shard_map/all_to_all | solution.py:18
  160.9 4.6 %all-to-all-done.6 = bf16[4,8,1664]{2,1,0:T(8,128)(2,1)S(1)} async-done(((bf16[4,8,1664]{2,1,0:T(8,128)(2,1)}), bf16[4,8,1664]{2,1,0:T(8,128)(2,1)S(1)}, u32[]{:S(2)}, u32[]{:S(2)}) %all-to-all-start.6) | async-done | bytes 106528 | tf_op jit(solution)/shard_map/all_to_all | solution.py:18
  165.5 0.2 fusion.56
  165.9 0.1 fusion.47
  166.0 0.1 add_divide_fusion
  166.1 0.1 copy.80
  166.3 2.0 fusion.1
  168.4 0.7 multiply_add_fusion
  169.2 1.3 copy-done.1
  170.5 1.9 fusion.65
  172.3 0.1 fusion.43
  172.5 0.6 broadcast_in_dim.98
  173.1 3.3 %all-to-all-start.7 = ((bf16[4,8,512]{2,1,0:T(8,128)(2,1)}), bf16[4,8,512]{2,1,0:T(8,128)(2,1)S(1)}, u32[]{:S(2)}, u32[]{:S(2)}) async-start(bf16[4,8,512]{2,1,0:T(8,128)(2,1)} %broadcast_in_dim.98), calls=%async_computation.7 | async-start | bytes 65536 | tf_op jit(solution)/shard_map/all_to_all | solution.py:18
  176.5 4.2 %all-to-all-done.7 = bf16[4,8,512]{2,1,0:T(8,128)(2,1)S(1)} async-done(((bf16[4,8,512]{2,1,0:T(8,128)(2,1)}), bf16[4,8,512]{2,1,0:T(8,128)(2,1)S(1)}, u32[]{:S(2)}, u32[]{:S(2)}) %all-to-all-start.7) | async-done | bytes 32800 | tf_op jit(solution)/shard_map/all_to_all | solution.py:18
  180.7 0.2 stack.6
  180.9 64.1 %all_to_all.55 = bf16[8,64,2624]{2,1,0:T(8,128)(2,1)S(1)} all-to-all(bf16[8,64,2624]{2,1,0:T(8,128)(2,1)S(1)} %stack.6), channel_id=1, replica_groups=mesh['z'=8,'y'=4,'x'=4,'c'=2] {'z'}, dimensions={0} | all-to-all | bytes 5373952 | tf_op jit(solution)/shard_map/all_to_all | solution.py:146
  245.0 0.2 convolution_convert_fusion.4
  245.3 13.4 %all_to_all.56 = bf16[8,32,512]{2,1,0:T(8,128)(2,1)S(1)} all-to-all(bf16[8,32,512]{2,1,0:T(8,128)(2,1)S(1)} %broadcast_in_dim.99), channel_id=1, replica_groups=mesh['z'=8,'y'=4,'x'=4,'c'=2] {'x','c'}, dimensions={0} | all-to-all | bytes 524288 | tf_op jit(solution)/shard_map/all_to_all | solution.py:18
  258.7 0.1 multiply_reduce_fusion
  258.8 0.3 convolution_convert_fusion
  259.3 0.8 broadcast_in_dim.102
  260.1 3.5 %all-to-all-start.9 = ((bf16[4,32,1536]{2,1,0:T(8,128)(2,1)}), bf16[4,32,1536]{2,1,0:T(8,128)(2,1)S(1)}, u32[]{:S(2)}, u32[]{:S(2)}) async-start(bf16[4,32,1536]{2,1,0:T(8,128)(2,1)} %broadcast_in_dim.102), calls=%async_computation.9 | async-start | bytes 786432 | tf_op jit(solution)/shard_map/all_to_all | solution.py:18
  263.6 6.8 %all-to-all-done.9 = bf16[4,32,1536]{2,1,0:T(8,128)(2,1)S(1)} async-done(((bf16[4,32,1536]{2,1,0:T(8,128)(2,1)}), bf16[4,32,1536]{2,1,0:T(8,128)(2,1)S(1)}, u32[]{:S(2)}, u32[]{:S(2)}) %all-to-all-start.9) | async-done | bytes 393248 | tf_op jit(solution)/shard_map/all_to_all | solution.py:18
  270.4 0.2 fusion.36
  270.6 0.4 convolution_convert_fusion.2
  271.0 0.1 copy.83
  271.1 0.2 reshape.158
  271.3 15.5 %all_to_all.57 = bf16[64,2,256]{2,1,0:T(2,128)(2,1)S(1)} all-to-all(bf16[64,2,256]{2,1,0:T(2,128)(2,1)S(1)} %reshape.158), channel_id=1, replica_groups=mesh['z'=8,'y'=4,'x'=4,'c'=2] {'z','x','c'}, dimensions={0} | all-to-all | bytes 131072 | tf_op jit(solution)/shard_map/all_to_all | solution.py:18
  286.8 0.1 reshape.159
  287.1 0.7 convert_element_type.213
  (76 shorter events, 1.5 us)
Async XLA Ops:
  2.2 22.3 %all-to-all-start.1 = ((bf16[64,2,128]{2,1,0:T(2,128)(2,1)}), bf16[64,2,128]{2,1,0:T(2,128)(2,1)S(1)}, u32[]{:S(2)}, u32[]{:S(2)}) async-start(bf16[64,2,128]{2,1,0:T(2,128)(2,1)} %reshape.156), calls=%async_computation.1 | async-start | bytes 65536 | tf_op jit(solution)/shard_map/all_to_all | solution.py:18
  16.2 14.2 %copy-start.7 = (bf16[64,512]{1,0:T(8,128)(2,1)S(1)}, bf16[64,512]{1,0:T(8,128)(2,1)}, u32[]{:S(2)}) copy-start(bf16[64,512]{1,0:T(8,128)(2,1)} %param.30) | copy-start | bytes 196612
  16.2 14.2 %copy-start.8 = (bf16[64,512]{1,0:T(8,128)(2,1)S(1)}, bf16[64,512]{1,0:T(8,128)(2,1)}, u32[]{:S(2)}) copy-start(bf16[64,512]{1,0:T(8,128)(2,1)} %param.31) | copy-start | bytes 196612
  16.2 14.2 %copy-start.10 = (bf16[64,256]{1,0:T(8,128)(2,1)S(1)}, bf16[64,256]{1,0:T(8,128)(2,1)}, u32[]{:S(2)}) copy-start(bf16[64,256]{1,0:T(8,128)(2,1)} %param.28) | copy-start | bytes 98308
  16.3 14.2 %copy-start.11 = (bf16[64,256]{1,0:T(8,128)(2,1)S(1)}, bf16[64,256]{1,0:T(8,128)(2,1)}, u32[]{:S(2)}) copy-start(bf16[64,256]{1,0:T(8,128)(2,1)} %param.29) | copy-start | bytes 98308
  25.7 4.8 %copy-start.12 = (f32[64]{0:T(128)S(1)}, f32[64]{0:T(128)}, u32[]{:S(2)}) copy-start(f32[64]{0:T(128)} %param.27) | copy-start | bytes 772
  25.7 39.5 %all-to-all-start.2 = ((bf16[8,64,1408]{2,1,0:T(8,128)(2,1)}), bf16[8,64,1408]{2,1,0:T(8,128)(2,1)S(1)}, u32[]{:S(2)}, u32[]{:S(2)}) async-start(bf16[8,64,1408]{2,1,0:T(8,128)(2,1)} %stack.7), calls=%async_computation.2 | async-start | bytes 2883584 | tf_op jit(solution)/shard_map/all_to_all | solution.py:146
  30.4 40.1 %copy-start.3 = (bf16[704,64]{0,1:T(8,128)(2,1)S(1)}, bf16[704,64]{0,1:T(8,128)(2,1)}, u32[]{:S(2)}) copy-start(bf16[704,64]{0,1:T(8,128)(2,1)} %param.26) | copy-start | bytes 270340
  66.4 10.4 %all-to-all-start.3 = ((bf16[4,32,1536]{2,1,0:T(8,128)(2,1)}), bf16[4,32,1536]{2,1,0:T(8,128)(2,1)S(1)}, u32[]{:S(2)}, u32[]{:S(2)}) async-start(bf16[4,32,1536]{2,1,0:T(8,128)(2,1)} %broadcast_in_dim.91), calls=%async_computation.3 | async-start | bytes 786432 | tf_op jit(solution)/shard_map/all_to_all | solution.py:18
  78.4 61.3 %all-to-all-start.4 = ((bf16[8,64,2368]{2,1,0:T(8,128)(2,1)}), bf16[8,64,2368]{2,1,0:T(8,128)(2,1)S(1)}, u32[]{:S(2)}, u32[]{:S(2)}) async-start(bf16[8,64,2368]{2,1,0:T(8,128)(2,1)} %stack.8), calls=%async_computation.4 | async-start | bytes 4980736 | tf_op jit(solution)/shard_map/all_to_all | solution.py:146
  82.3 65.5 %copy-start.4 = (bf16[64,704]{1,0:T(8,128)(2,1)S(1)}, bf16[64,704]{1,0:T(8,128)(2,1)}, u32[]{:S(2)}) copy-start(bf16[64,704]{1,0:T(8,128)(2,1)} %param.40) | copy-start | bytes 270340
  82.3 65.5 %copy-start.5 = (bf16[64,704]{1,0:T(8,128)(2,1)S(1)}, bf16[64,704]{1,0:T(8,128)(2,1)}, u32[]{:S(2)}) copy-start(bf16[64,704]{1,0:T(8,128)(2,1)} %param.39) | copy-start | bytes 270340
  82.3 65.4 %copy-start.13 = (f32[64]{0:T(128)S(1)}, f32[64]{0:T(128)}, u32[]{:S(2)}) copy-start(f32[64]{0:T(128)} %param.38) | copy-start | bytes 772
  139.7 1.6 copy-start.2
  141.1 19.8 %copy-start.16 = (f32[4]{0:T(128)S(1)}, f32[4]{0:T(128)}, u32[]{:S(2)}) copy-start(f32[4]{0:T(128)} %param.34) | copy-start | bytes 52
  141.1 24.9 %copy-start.15 = (f32[4]{0:T(128)S(1)}, f32[4]{0:T(128)}, u32[]{:S(2)}) copy-start(f32[4]{0:T(128)} %param.35) | copy-start | bytes 52
  141.2 13.0 %all-to-all-start.5 = ((bf16[8,32,512]{2,1,0:T(8,128)(2,1)}), bf16[8,32,512]{2,1,0:T(8,128)(2,1)S(1)}, u32[]{:S(2)}, u32[]{:S(2)}) async-start(bf16[8,32,512]{2,1,0:T(8,128)(2,1)} %broadcast_in_dim.93), calls=%async_computation.5 | async-start | bytes 524288 | tf_op jit(solution)/shard_map/all_to_all | solution.py:18
  147.8 18.5 %copy-start = (f32[8,4,128,128]{3,2,1,0:T(8,128)S(1)}, f32[8,4,128,128]{3,2,1,0:T(8,128)}, u32[]{:S(2)}) copy-start(f32[8,4,128,128]{3,2,1,0:T(8,128)} %param.22) | copy-start | bytes 6291460
  157.5 8.0 %all-to-all-start.6 = ((bf16[4,8,1664]{2,1,0:T(8,128)(2,1)}), bf16[4,8,1664]{2,1,0:T(8,128)(2,1)S(1)}, u32[]{:S(2)}, u32[]{:S(2)}) async-start(bf16[4,8,1664]{2,1,0:T(8,128)(2,1)} %pad_maximum_fusion.2), calls=%async_computation.6 | async-start | bytes 212992 | tf_op jit(solution)/shard_map/all_to_all | solution.py:18
  169.1 1.3 copy-start.1
  169.2 3.3 %copy-start.14 = (f32[128]{0:T(128)S(1)}, f32[128]{0:T(128)}, u32[]{:S(2)}) copy-start(f32[128]{0:T(128)} %param.36) | copy-start | bytes 1540
  169.2 7.2 %copy-start.6 = (bf16[704,64]{0,1:T(8,128)(2,1)S(1)}, bf16[704,64]{0,1:T(8,128)(2,1)}, u32[]{:S(2)}) copy-start(bf16[704,64]{0,1:T(8,128)(2,1)} %param.41) | copy-start | bytes 270340
  169.2 7.2 %copy-start.9 = (bf16[512,64]{0,1:T(8,128)(2,1)S(1)}, bf16[512,64]{0,1:T(8,128)(2,1)}, u32[]{:S(2)}) copy-start(bf16[512,64]{0,1:T(8,128)(2,1)} %param.37) | copy-start | bytes 196612
  173.1 7.5 %all-to-all-start.7 = ((bf16[4,8,512]{2,1,0:T(8,128)(2,1)}), bf16[4,8,512]{2,1,0:T(8,128)(2,1)S(1)}, u32[]{:S(2)}, u32[]{:S(2)}) async-start(bf16[4,8,512]{2,1,0:T(8,128)(2,1)} %broadcast_in_dim.98), calls=%async_computation.7 | async-start | bytes 65536 | tf_op jit(solution)/shard_map/all_to_all | solution.py:18
  260.1 10.3 %all-to-all-start.9 = ((bf16[4,32,1536]{2,1,0:T(8,128)(2,1)}), bf16[4,32,1536]{2,1,0:T(8,128)(2,1)S(1)}, u32[]{:S(2)}, u32[]{:S(2)}) async-start(bf16[4,32,1536]{2,1,0:T(8,128)(2,1)} %broadcast_in_dim.102), calls=%async_computation.9 | async-start | bytes 786432 | tf_op jit(solution)/shard_map/all_to_all | solution.py:18
